TPU v7x, 256 devices: a whole 4x4x8 slice. The times are simulated.
256 devices in a mesh: ep: 64 (over z, y, core), tp: 4 (over x).
Axes of the slice: x: 4, y: 4, z: 8, core: 2. Of those that a mesh axis runs over, the one named last changes fastest.
Arguments:
- mixer_input: bfloat16 [32768, 2048], P(('ep', 'tp')), may hold values from -6 to 6
- expert_input: bfloat16 [32768, 2048], P(('ep', 'tp')), may hold values from -6 to 6
- mixer_gain: float32 [2048], replicated, may hold values from 0.1 to 1.9
- expert_gain: float32 [2048], replicated, may hold values from 0.1 to 1.9
- query_weight: bfloat16 [2048, 1024], P(None, 'tp'), may hold values from -0.125 to 0.125
- key_weight: bfloat16 [2048, 1024], P(None, 'tp'), may hold values from -0.125 to 0.125
- value_weight: bfloat16 [2048, 1024], P(None, 'tp'), may hold values from -0.125 to 0.125
- out_weight: bfloat16 [1024, 2048], P('tp'), may hold values from -0.1875 to 0.1875
- decay_rate: float32 [8], P('tp'), may hold values from 0 to 0.12
- routing: int32 [32768, 4], P('ep'), may hold values from 0 to 63, all different within a row; in each aligned block of 128 rows (0 to 127, 128 to 255, ...) at most 12 rows name the same one
- route_weight: float32 [32768, 4], P('ep'), may hold values from 0.2 to 1
- gate_weight: bfloat16 [64, 2048, 1024], P('ep', None, 'tp'), may hold values from -0.125 to 0.125
- up_weight: bfloat16 [64, 2048, 1024], P('ep', None, 'tp'), may hold values from -0.125 to 0.125
- down_weight: bfloat16 [64, 1024, 2048], P('ep', None, 'tp'), may hold values from -0.1875 to 0.1875
- shared_gate: bfloat16 [2048, 512], P(None, 'tp'), may hold values from -0.125 to 0.125
- shared_up: bfloat16 [2048, 512], P(None, 'tp'), may hold values from -0.125 to 0.125
- shared_down: bfloat16 [512, 2048], P(None, 'tp'), may hold values from -0.25 to 0.25
Outputs:
- mixer_output: float32 [32768, 2048], P(('ep', 'tp'))
- expert_output: float32 [32768, 2048], P('ep', 'tp')
Inputs may be any that keep to these rules, and one draw needn't show every extreme that they name: `routing`: each row names 4 different experts. In each aligned block of 128 rows, no expert is named by more than 12 rows, and in some blocks one expert is named by exactly 12 rows.
All inputs are finite; a program needn't handle non-finite values.
Results may differ from a plain program's by a relative error of at most 0.0095.
Values may be sent and summed in bfloat16 or wider, within the bound.
A program may use at most 128 MiB of HBM per device.

v0:
```python
import jax
import jax.numpy as jnp
from jax import lax
from jax.sharding import Mesh
from jax.sharding import PartitionSpec as P

HD = 128
BLK = 64
EP = ("ep_0", "ep_1", "ep_2")
EP_TP = ("ep_0", "ep_1", "ep_2", "tp")


NORM_EPS = 1e-06
ROPE_BASE = 10000.0
EXACT_MATMUL = lax.Precision.HIGHEST


def nothing_yet(value, identity):
    return jax.tree.map(
        lambda a, e: jnp.broadcast_to(jnp.asarray(e, a.dtype), a.shape), value, identity
    )


def entering_2(value, axes, combine, identity):
    before = start = nothing_yet(value, identity)
    subtotal = value
    for axis in reversed(axes):
        count, mine = (lax.axis_size(axis), lax.axis_index(axis))
        pieces = jax.tree.map(lambda part: lax.all_gather(part, axis), subtotal)
        inside, subtotal = (start, start)
        for k in range(count):
            passed = k < mine
            subtotal = combine(subtotal, jax.tree.map(lambda part: part[k], pieces))
            inside = jax.tree.map(lambda new, old: jnp.where(passed, new, old), subtotal, inside)
        before = combine(inside, before)
    return before


def sent_together(arrays, axis, dim, along):
    ends, at = ([], 0)
    for a in arrays[:-1]:
        at += a.shape[along]
        ends.append(at)
    both = jnp.concatenate(arrays, axis=along)
    return tuple(jnp.split(lax.all_gather(both, axis, axis=dim, tiled=True), ends, axis=along))


def norm_rows(inputs, gain_vector):
    values = inputs.astype(jnp.float32)
    scaled = values * lax.rsqrt(jnp.mean(values * values, axis=-1, keepdims=True) + NORM_EPS)
    return (scaled * gain_vector).astype(jnp.bfloat16)


def rotate(head_rows, positions):
    head_size = head_rows.shape[-1]
    inverse = ROPE_BASE ** (-jnp.arange(0, head_size, 2, dtype=jnp.float32) / head_size)
    angles = positions[:, None] * inverse[None, :]
    cosine = jnp.cos(angles)[:, None, :]
    sine_part = jnp.sin(angles)[:, None, :]
    front_half = head_rows[..., : head_size // 2]
    behind = head_rows[..., head_size // 2 :]
    return jnp.concatenate(
        [front_half * cosine - behind * sine_part, front_half * sine_part + behind * cosine],
        axis=-1,
    )


def project(inputs, weight, head_total):
    product = jnp.dot(inputs, weight, preferred_element_type=jnp.float32).astype(jnp.bfloat16)
    product = lax.optimization_barrier(product)
    return product.astype(jnp.float32).reshape(inputs.shape[0], head_total, -1)


def chain_combine(earlier, latter):
    return (earlier[0] * latter[0], latter[0][:, None, None] * earlier[1] + latter[1])


def retain_local(query_heads, key_heads, value_heads, decay_rates):
    length, head_total, head_size = query_heads.shape
    blocks = length // BLK
    log_gamma = -decay_rates
    inner_pos = jnp.arange(BLK, dtype=jnp.float32)
    offsets = inner_pos[:, None] - inner_pos[None, :]
    inside_block_output = jnp.where(
        offsets >= 0, jnp.exp(log_gamma[:, None, None] * jnp.maximum(offsets, 0.0)), 0.0
    )
    key_scale = jnp.exp(log_gamma[None, :] * (BLK - 1.0 - inner_pos)[:, None])
    query_scale = jnp.exp(log_gamma[None, :] * (inner_pos + 1.0)[:, None])
    blocked = (blocks, BLK, head_total, head_size)
    q_blocks = query_heads.reshape(blocked)
    k_blocks = key_heads.reshape(blocked)
    v_blocks = value_heads.reshape(blocked)
    attention_scores = (
        jnp.einsum("nchd,nmhd->nhcm", q_blocks, k_blocks, precision=EXACT_MATMUL)
        * inside_block_output[None]
    )
    nearby = jnp.einsum("nhcm,nmhe->nche", attention_scores, v_blocks, precision=EXACT_MATMUL)
    block_states = jnp.einsum(
        "nchd,nche->nhde", k_blocks * key_scale[None, :, :, None], v_blocks, precision=EXACT_MATMUL
    )
    block_offset_rows = jnp.arange(blocks, dtype=jnp.float32)
    to_end = jnp.exp(log_gamma[None, :] * BLK * (blocks - 1.0 - block_offset_rows)[:, None])
    summary = jnp.einsum("nh,nhde->hde", to_end, block_states, precision=EXACT_MATMUL)
    through = jnp.exp(log_gamma * (BLK * blocks))
    incoming = entering_2(
        (through, summary), EP, chain_combine, (jnp.ones_like(through), jnp.zeros_like(summary))
    )[1]
    block_gaps = block_offset_rows[:, None] - 1.0 - block_offset_rows[None, :]
    carry_mix = jnp.where(
        block_gaps >= 0, jnp.exp(log_gamma[:, None, None] * BLK * jnp.maximum(block_gaps, 0.0)), 0.0
    )
    entering = jnp.einsum("hbj,jhde->bhde", carry_mix, block_states, precision=EXACT_MATMUL)
    entering = (
        entering
        + jnp.exp(log_gamma[None, :] * BLK * block_offset_rows[:, None])[:, :, None, None]
        * incoming[None]
    )
    distant = jnp.einsum(
        "bchd,bhde->bche",
        q_blocks * query_scale[None, :, :, None],
        entering,
        precision=EXACT_MATMUL,
    )
    retained = (nearby + distant).reshape(length, head_total, head_size)
    normed = retained * lax.rsqrt(jnp.mean(retained * retained, axis=-1, keepdims=True) + NORM_EPS)
    return normed.astype(jnp.bfloat16).reshape(length, head_total * head_size)


def assign_slots(routes, source_rows, capacity, expert_count):
    token_count, pick_count = routes.shape
    chosen = routes.reshape(token_count * pick_count)
    onehot = (chosen[:, None] == jnp.arange(expert_count, dtype=jnp.int32)[None, :]).astype(
        jnp.int32
    )
    per_source = onehot.reshape(token_count // source_rows, source_rows * pick_count, expert_count)
    earlier_hits = jnp.cumsum(per_source, axis=1) - per_source
    ranks = jnp.sum(earlier_hits * per_source, axis=2).reshape(token_count * pick_count)
    sources = jnp.arange(token_count * pick_count, dtype=jnp.int32) // (source_rows * pick_count)
    return (chosen, sources * capacity + ranks)


def gather_slots(token_rows, chosen, slot_ids, slot_count, expert_count, pick_count):
    owners = jnp.arange(chosen.shape[0], dtype=jnp.int32) // pick_count + 1
    owner_table = jnp.zeros((slot_count, expert_count), jnp.int32).at[slot_ids, chosen].set(owners)
    padded = jnp.concatenate(
        [jnp.zeros((1, token_rows.shape[1]), token_rows.dtype), token_rows], axis=0
    )
    return padded[owner_table]


def expert_hidden(routed_rows, gate_weight, up_weight):
    per_device = gate_weight.shape[0]
    grouped = routed_rows.reshape(
        routed_rows.shape[0], routed_rows.shape[1] // per_device, per_device, routed_rows.shape[2]
    )
    gate_part = jnp.einsum(
        "snxd,xdf->snxf", grouped, gate_weight, preferred_element_type=jnp.float32
    )
    up_part = jnp.einsum("snxd,xdf->snxf", grouped, up_weight, preferred_element_type=jnp.float32)
    return (jax.nn.silu(gate_part) * up_part).astype(jnp.bfloat16)


def shards(
    mixer_input,
    expert_input,
    mixer_gain,
    expert_gain,
    query_weight,
    key_weight,
    value_weight,
    out_weight,
    decay_rate,
    routing,
    route_weight,
    gate_weight,
    up_weight,
    down_weight,
    shared_gate,
    shared_up,
    shared_down,
):
    own_count = mixer_input.shape[0]
    tp_index = lax.axis_index("tp")
    own_expert_rows = norm_rows(expert_input, expert_gain)
    mixer_rows, expert_rows = sent_together(
        (norm_rows(mixer_input, mixer_gain), own_expert_rows), "tp", 0, 1
    )
    group_count = mixer_rows.shape[0]
    head_total = decay_rate.shape[0]
    positions = (
        lax.axis_index(EP) * group_count + jnp.arange(group_count, dtype=jnp.int32)
    ).astype(jnp.float32)
    query_heads = rotate(project(mixer_rows, query_weight, head_total), positions) * HD ** (-0.5)
    key_heads = rotate(project(mixer_rows, key_weight, head_total), positions)
    value_heads = project(mixer_rows, value_weight, head_total)
    mixed_heads = retain_local(query_heads, key_heads, value_heads, decay_rate)
    mixer_output = lax.psum_scatter(
        jnp.dot(mixed_heads, out_weight, preferred_element_type=jnp.float32).astype(jnp.bfloat16),
        "tp",
        scatter_dimension=0,
        tiled=True,
    ).astype(jnp.float32)
    expert_count = lax.axis_size(EP) * gate_weight.shape[0]
    pick_count = routing.shape[1]
    capacity = (3 * own_count * pick_count + 2 * expert_count - 1) // (2 * expert_count)
    chosen, slot_ids = assign_slots(routing, own_count, capacity, expert_count)
    own_span = own_count * pick_count
    own_chosen = lax.dynamic_slice_in_dim(chosen, tp_index * own_span, own_span, 0)
    own_slots = (
        lax.dynamic_slice_in_dim(slot_ids, tp_index * own_span, own_span, 0) - tp_index * capacity
    )
    outgoing = gather_slots(
        own_expert_rows, own_chosen, own_slots, capacity, expert_count, pick_count
    )
    arrived = lax.all_to_all(outgoing, EP, split_axis=1, concat_axis=1, tiled=True)
    hidden = expert_hidden(
        lax.all_gather(arrived, "tp", axis=0, tiled=True), gate_weight, up_weight
    )
    shared_hidden = (
        jax.nn.silu(jnp.dot(expert_rows, shared_gate, preferred_element_type=jnp.float32))
        * jnp.dot(expert_rows, shared_up, preferred_element_type=jnp.float32)
    ).astype(jnp.bfloat16)
    full_hidden, full_shared = (
        lax.all_gather(hidden, "tp", axis=3, tiled=True),
        lax.all_gather(shared_hidden, "tp", axis=1, tiled=True),
    )
    results = jnp.einsum(
        "snxf,xfe->snxe", full_hidden, down_weight, preferred_element_type=jnp.float32
    ).astype(jnp.bfloat16)
    results = results.reshape(results.shape[0], expert_count, results.shape[3])
    returned = lax.all_to_all(results, EP, split_axis=1, concat_axis=1, tiled=True)
    flat_results = returned.reshape(returned.shape[0] * expert_count, returned.shape[2])
    picked = flat_results[slot_ids * expert_count + chosen].astype(jnp.float32)
    weighted = jnp.sum(
        picked.reshape(group_count, pick_count, -1) * route_weight[:, :, None], axis=1
    )
    shared_result = jnp.dot(full_shared, shared_down, preferred_element_type=jnp.float32)
    expert_output = weighted + shared_result
    return (mixer_output, expert_output)


def solution(mesh):
    finer = Mesh(mesh.devices.reshape(8, 4, 2, mesh.shape["tp"]), ("ep_0", "ep_1", "ep_2", "tp"))
    placed = (
        P(EP_TP, None),
        P(EP_TP, None),
        P(),
        P(),
        P(None, "tp"),
        P(None, "tp"),
        P(None, "tp"),
        P("tp", None),
        P("tp"),
        P(EP, None),
        P(EP, None),
        P(EP, None, "tp"),
        P(EP, None, "tp"),
        P(EP, None, "tp"),
        P(None, "tp"),
        P(None, "tp"),
        P(None, "tp"),
    )
    return jax.shard_map(
        shards,
        mesh=finer,
        in_specs=placed,
        out_specs=(P(EP_TP, None), P(EP, "tp")),
        check_vma=False,
    )
```

profile of v0, /device:TPU:1, one launch (start us, length us, event | category | flops | bytes accessed | tf_op | source)
XLA Modules:
  0.0 539.3 jit_solution(6858122981832166352)
XLA Ops:
  8.7 1.2 fusion.36
  9.9 1.2 fusion.39
  11.3 4.8 reduce-window.6
  17.0 25.4 %scatter_fusion = s32[12,64]{1,0:T(8,128)S(1)} fusion(s32[12,64]{1,0:T(8,128)S(1)} %broadcast.456, s32[512]{0:T(512)S(1)} %bitcast.156, s32[512]{0:T(512)S(1)} %fusion.96), kind=kCustom, calls=%fused_computation.2 | custom fusion | bytes 10240 | tf_op jit(solution)/shard_map/scatter | solution.py:144
  42.5 1.0 fusion.38
  43.6 4.3 gather_fusion
  47.9 3.7 copy.112
  51.5 107.6 %all_to_all.10 = bf16[12,64,2048]{2,0,1:T(8,128)(2,1)S(1)} all-to-all(bf16[12,64,2048]{2,0,1:T(8,128)(2,1)S(1)} %copy.112), channel_id=1, replica_groups=mesh['ep_0'=8,'ep_1'=4,'ep_2'=2,'tp'=4] {'ep_0','ep_1','ep_2'}, dimensions={1} | all-to-all | bytes 6291456 | tf_op jit(solution)/shard_map/all_to_all | solution.py:215
  159.1 3.4 copy.113
  162.6 1.0 copy-done.9
  163.5 1.0 pad_maximum_fusion
  164.8 116.4 %all-gather.13.cloned.1.call-done = bf16[48,64,2048]{2,1,0:T(8,128)(2,1)} async-done(((bf16[12,64,2048]{2,1,0:T(8,128)(2,1)}), bf16[48,64,2048]{2,1,0:T(8,128)(2,1)}) %all-gather.13.cloned.1.call-update) | async-done | bytes 12582928 | tf_op jit(solution)/shard_map/all_gather | solution.py:217
  281.2 7.9 %fusion.43 = f32[48,64,256]{2,1,0:T(8,128)S(1)} fusion(bf16[48,64,2048]{2,1,0:T(8,128)(2,1)} %all-gather.13.cloned.1.call-done, bf16[1,2048,256]{2,1,0:T(8,128)(2,1)} %param.29), kind=kOutput, calls=%fused_computation.48 | convolution fusion | flops 3221225472 | bytes 16777216 | tf_op jit(solution)/shard_map/snxd,xdf->snxf/dot_general | solution.py:159
  289.7 5.1 fusion.2
  296.3 2.9 all-reduce.1
  300.6 9.2 %all-reduce.2 = f32[8]{0:T(128)S(1)} all-reduce(f32[8]{0:T(128)S(1)} %get-tuple-element.36), channel_id=4, replica_groups=mesh['ep_0'=8,'ep_1'=4,'ep_2'=2,'tp'=4] {'ep_1'}, use_global_device_ids=true, to_apply=%add.2 | all-reduce | flops 8 | bytes 64
  310.5 14.4 %all-gather.3 = f32[8,1,2]{2,1,0:T(1,128)S(1)} all-gather(f32[1,1,2]{2,1,0:T(1,128)S(1)} %get-tuple-element.28), channel_id=1, replica_groups=mesh['ep_0'=8,'ep_1'=4,'ep_2'=2,'tp'=4] {'ep_0'}, dimensions={0}, use_global_device_ids=true | all-gather | bytes 72 | tf_op jit(solution)/shard_map/all_gather | solution.py:29
  327.1 1.7 multiply_cosine_fusion
  328.8 6.5 %all-gather.9.cloned.1.call-done = bf16[512,4096]{1,0:T(8,128)(2,1)} async-done(((bf16[128,4096]{1,0:T(8,128)(2,1)}), bf16[512,4096]{1,0:T(8,128)(2,1)}) %all-gather.9.cloned.1.call-update) | async-done | bytes 4194320 | tf_op jit(solution)/shard_map/all_gather | solution.py:45
  335.3 2.6 fusion.24
  338.2 2.6 fusion.27
  341.0 2.6 fusion.21
  344.9 1.2 multiply_subtract_fusion.1
  346.3 1.1 fusion.54
  347.4 1.5 fusion.47
  348.9 2.7 all-gather.1
  352.4 11.5 %all_gather.47 = f32[4,2,128,128]{3,2,1,0:T(8,128)S(1)} all-gather(f32[1,2,128,128]{3,2,1,0:T(8,128)S(1)} %fusion.72), channel_id=1, replica_groups=mesh['ep_0'=8,'ep_1'=4,'ep_2'=2,'tp'=4] {'ep_1'}, dimensions={0}, use_global_device_ids=true | all-gather | bytes 655360 | tf_op jit(solution)/shard_map/all_gather | solution.py:29
  364.8 43.1 %all-gather.15.cloned.1.call-done = bf16[48,64,1,1024]{3,1,0,2:T(8,128)(2,1)} async-done(((bf16[48,64,1,256]{3,1,0,2:T(8,128)(2,1)}), bf16[48,64,1,1024]{3,1,0,2:T(8,128)(2,1)}) %all-gather.15.cloned.1.call-update) | async-done | bytes 6291472 | tf_op jit(solution)/shard_map/all_gather | solution.py:224
  407.9 6.4 %fusion.6 = bf16[48,64,512]{2,1,0:T(8,128)(2,1)S(1)} fusion(bf16[48,64,1,1024]{3,1,0,2:T(8,128)(2,1)} %all-gather.15.cloned.1.call-done, bf16[1,1024,512]{2,1,0:T(8,128)(2,1)S(1)} %copy-done), kind=kOutput, calls=%fused_computation.14 | convolution fusion | flops 3222798336 | bytes 10485760 | tf_op jit(solution)/shard_map/snxf,xfe->snxe/dot_general | solution.py:227
  414.3 3.4 copy.114
  417.8 12.5 %all-to-all-start.1 = ((bf16[48,64,512]{2,0,1:T(8,128)(2,1)}), bf16[48,64,512]{2,0,1:T(8,128)(2,1)}, u32[]{:S(2)}, u32[]{:S(2)}) async-start(bf16[48,64,512]{2,0,1:T(8,128)(2,1)} %copy.114), calls=%async_computation.2 | async-start | bytes 6291456 | tf_op jit(solution)/shard_map/all_to_all | solution.py:231
  431.0 2.2 convolution_multiply_fusion
  433.3 2.2 fusion.66
  435.5 19.0 %all-gather.11.cloned.1.call-done = f32[8,2,128,128]{3,2,1,0:T(8,128)} async-done(((f32[1,2,128,128]{3,2,1,0:T(8,128)}), f32[8,2,128,128]{3,2,1,0:T(8,128)}) %all-gather.11.cloned.1.call-update) | async-done | bytes 1048592 | tf_op jit(solution)/shard_map/all_gather | solution.py:29
  454.6 1.8 fusion.71
  456.4 1.6 fusion.19
  458.1 1.3 multiply_reduce_fusion.1
  460.6 3.4 convolution_convert_fusion
  464.5 2.3 fusion.11
  466.8 2.3 fusion.33
  469.1 16.4 %all_gather.51 = bf16[512,512]{1,0:T(8,128)(2,1)} all-gather(bf16[512,128]{1,0:T(8,128)(2,1)S(1)} %fusion.33), channel_id=1, replica_groups=mesh['ep_0'=8,'ep_1'=4,'ep_2'=2,'tp'=4] {'tp'}, dimensions={1}, use_global_device_ids=true | all-gather | bytes 655360 | tf_op jit(solution)/shard_map/all_gather | solution.py:225
  485.5 19.6 %reduce-scatter.2.cloned.1.call-done = bf16[128,2048]{1,0:T(8,128)(2,1)} async-done(((bf16[512,2048]{1,0:T(8,128)(2,1)}), bf16[128,2048]{1,0:T(8,128)(2,1)}) %reduce-scatter.2.cloned.1.call-update) | async-done | bytes 524304 | tf_op jit(solution)/shard_map/reduce_scatter | solution.py:197
  505.1 2.1 convert_element_type.78
  507.8 5.3 copy.115
  513.2 9.9 %gather_fusion.1 = bf16[2048,512]{1,0:T(8,128)(2,1)S(1)} fusion(bf16[3072,512]{1,0:T(8,128)(2,1)} %bitcast.155, s32[2048]{0:T(1024)S(1)} %broadcast_clamp_fusion), kind=kCustom, calls=%fused_computation.1 | custom fusion | bytes 4202496 | tf_op jit(solution)/shard_map/gather | solution.py:233
  523.0 3.0 reshape.473
  526.1 4.9 multiply_reduce_fusion
  530.9 1.4 convolution_add_fusion
  (142 shorter events, 14.4 us)
Async XLA Ops:
  7.2 400.7 %copy-start = (bf16[1,1024,512]{2,1,0:T(8,128)(2,1)S(1)}, bf16[1,1024,512]{2,1,0:T(8,128)(2,1)}, u32[]{:S(2)}) copy-start(bf16[1,1024,512]{2,1,0:T(8,128)(2,1)} %param.30) | copy-start | bytes 3145732
  7.2 274.0 %all-gather.13.cloned.1.call-start = ((), (), s32[]{:S(2)}) async-start(), calls=%async_computation.6 | async-start | bytes 15728640 | tf_op jit(solution)/shard_map/all_gather | solution.py:217
  11.2 31.2 %copy-start.6 = (bf16[128,2048]{1,0:T(8,128)(2,1)S(1)}, bf16[128,2048]{1,0:T(8,128)(2,1)}, u32[]{:S(2)}) copy-start(bf16[128,2048]{1,0:T(8,128)(2,1)} %param.17) | copy-start | bytes 1572868
  11.2 31.2 %copy-start.12 = (f32[2048]{0:T(1024)S(1)}, f32[2048]{0:T(1024)}, u32[]{:S(2)}) copy-start(f32[2048]{0:T(1024)} %param.19) | copy-start | bytes 24580
  11.2 31.2 %copy-start.13 = (f32[2048]{0:T(1024)S(1)}, f32[2048]{0:T(1024)}, u32[]{:S(2)}) copy-start(f32[2048]{0:T(1024)} %param.20) | copy-start | bytes 24580
  16.0 26.4 %copy-start.7 = (bf16[128,2048]{1,0:T(8,128)(2,1)S(1)}, bf16[128,2048]{1,0:T(8,128)(2,1)}, u32[]{:S(2)}) copy-start(bf16[128,2048]{1,0:T(8,128)(2,1)} %param.18) | copy-start | bytes 1572868
  162.5 1.0 copy-start.9
  162.5 172.8 %all-gather.9.cloned.1.call-start = ((), (), s32[]{:S(2)}) async-start(), calls=%async_computation.3 | async-start | bytes 5242880 | tf_op jit(solution)/shard_map/all_gather | solution.py:45
  164.6 124.5 %copy-start.32 = (bf16[1,2048,256]{2,1,0:T(8,128)(2,1)S(1)}, bf16[1,2048,256]{2,1,0:T(8,128)(2,1)}, u32[]{:S(2)}) copy-start(bf16[1,2048,256]{2,1,0:T(8,128)(2,1)} %param.28) | copy-start | bytes 3145732
  164.6 243.3 %all-gather.15.cloned.1.call-start = ((), (), s32[]{:S(2)}) async-start(), calls=%async_computation.7 | async-start | bytes 7864320 | tf_op jit(solution)/shard_map/all_gather | solution.py:224
  281.2 8.5 %copy-start.31 = (bf16[48,64,2048]{2,1,0:T(8,128)(2,1)S(1)}, bf16[48,64,2048]{2,1,0:T(8,128)(2,1)}, u32[]{:S(2)}) copy-start(bf16[48,64,2048]{2,1,0:T(8,128)(2,1)} %all-gather.13.cloned.1.call-done) | copy-start | bytes 37748740
  289.7 5.2 copy-start.36
  289.7 6.5 %copy-start.28 = (f32[2]{0:T(128)S(1)}, f32[2]{0:T(128)}, u32[]{:S(2)}) copy-start(f32[2]{0:T(128)} %param.25) | copy-start | bytes 28
  289.7 9.6 %copy-start.35 = (u32[256]{0:T(256)S(1)}, u32[256]{0:T(256)}, u32[]{:S(2)}) copy-start(u32[256]{0:T(256)} %constant.162) | copy-start | bytes 3076
  294.8 159.7 %all-gather.11.cloned.1.call-start = ((), (), s32[]{:S(2)}) async-start(), calls=%async_computation.4 | async-start | bytes 1179648 | tf_op jit(solution)/shard_map/all_gather | solution.py:29
  296.3 41.6 %copy-start.15 = (f32[2]{0:T(128)}, f32[2]{0:T(128)S(1)}, u32[]{:S(2)}) copy-start(f32[2]{0:T(128)S(1)} %get-tuple-element.39) | copy-start | bytes 28
  325.0 12.9 %copy-start.29 = (f32[8]{0:T(128)}, f32[8]{0:T(128)S(1)}, u32[]{:S(2)}) copy-start(f32[8]{0:T(128)S(1)} %iota_add_fusion.2) | copy-start | bytes 100
  343.6 2.7 copy-start.3
  343.6 1.2 copy-start.10
  351.6 0.7 copy-start.4
  417.7 12.6 %copy-start.30 = (f32[8]{0:T(128)S(1)}, f32[8]{0:T(128)}, u32[]{:S(2)}) copy-start(f32[8]{0:T(128)} %copy-done.29) | copy-start | bytes 100
  417.8 90.1 %all-to-all-start.1 = ((bf16[48,64,512]{2,0,1:T(8,128)(2,1)}), bf16[48,64,512]{2,0,1:T(8,128)(2,1)}, u32[]{:S(2)}, u32[]{:S(2)}) async-start(bf16[48,64,512]{2,0,1:T(8,128)(2,1)} %copy.114), calls=%async_computation.2 | async-start | bytes 6291456 | tf_op jit(solution)/shard_map/all_to_all | solution.py:231
  430.2 24.3 %copy-start.19 = (f32[2]{0:T(128)S(1)}, f32[2]{0:T(128)}, u32[]{:S(2)}) copy-start(f32[2]{0:T(128)} %get-tuple-element.31) | copy-start | bytes 28
  430.3 24.3 %copy-start.20 = (f32[2]{0:T(128)S(1)}, f32[2]{0:T(128)}, u32[]{:S(2)}) copy-start(f32[2]{0:T(128)} %get-tuple-element.32) | copy-start | bytes 28
  430.3 24.3 %copy-start.21 = (f32[2]{0:T(128)S(1)}, f32[2]{0:T(128)}, u32[]{:S(2)}) copy-start(f32[2]{0:T(128)} %get-tuple-element.14) | copy-start | bytes 28
  430.3 24.3 %copy-start.22 = (f32[2]{0:T(128)S(1)}, f32[2]{0:T(128)}, u32[]{:S(2)}) copy-start(f32[2]{0:T(128)} %get-tuple-element.15) | copy-start | bytes 28
  430.3 24.3 %copy-start.23 = (f32[2]{0:T(128)S(1)}, f32[2]{0:T(128)}, u32[]{:S(2)}) copy-start(f32[2]{0:T(128)} %get-tuple-element.16) | copy-start | bytes 28
  430.3 24.3 %copy-start.24 = (f32[2]{0:T(128)S(1)}, f32[2]{0:T(128)}, u32[]{:S(2)}) copy-start(f32[2]{0:T(128)} %get-tuple-element.17) | copy-start | bytes 28
  430.3 24.3 %copy-start.25 = (f32[2]{0:T(128)S(1)}, f32[2]{0:T(128)}, u32[]{:S(2)}) copy-start(f32[2]{0:T(128)} %get-tuple-element.18) | copy-start | bytes 28
  430.3 24.3 %copy-start.26 = (f32[2]{0:T(128)S(1)}, f32[2]{0:T(128)}, u32[]{:S(2)}) copy-start(f32[2]{0:T(128)} %get-tuple-element.19) | copy-start | bytes 28
  430.3 26.1 %copy-start.16 = (f32[2]{0:T(128)S(1)}, f32[2]{0:T(128)}, u32[]{:S(2)}) copy-start(f32[2]{0:T(128)} %copy-done.15) | copy-start | bytes 28
  430.3 26.1 %copy-start.18 = (f32[8,2]{0,1:T(2,128)S(1)}, f32[8,2]{0,1:T(2,128)}, u32[]{:S(2)}) copy-start(f32[8,2]{0,1:T(2,128)} %get-tuple-element.26) | copy-start | bytes 196
  430.3 74.8 %reduce-scatter.2.cloned.1.call-start = ((), (), s32[]{:S(2)}) async-start(), calls=%async_computation.5 | async-start | bytes 2621440 | tf_op jit(solution)/shard_map/reduce_scatter | solution.py:197
  433.3 23.1 %copy-start.27 = (pred[8,8]{1,0:T(8,128)(4,1)S(1)}, pred[8,8]{1,0:T(8,128)(4,1)}, u32[]{:S(2)}) copy-start(pred[8,8]{1,0:T(8,128)(4,1)} %fusion.90) | copy-start | bytes 196
  433.3 24.8 %copy-start.1 = (f32[512,2,64]{2,0,1:T(8,128)S(1)}, f32[512,2,64]{2,0,1:T(8,128)}, u32[]{:S(2)}) copy-start(f32[512,2,64]{2,0,1:T(8,128)} %get-tuple-element.4) | copy-start | bytes 786436
  433.3 24.8 %copy-start.17 = (f32[64,2]{0,1:T(2,128)S(1)}, f32[64,2]{0,1:T(2,128)}, u32[]{:S(2)}) copy-start(f32[64,2]{0,1:T(2,128)} %get-tuple-element.24) | copy-start | bytes 1540
  454.5 3.6 copy-start.2
  454.5 3.6 copy-start.8
  460.6 3.7 copy-start.14
  460.6 3.9 copy-start.33
  464.1 2.7 copy-start.34
  526.1 4.9 copy-start.5
  526.1 4.9 copy-start.11
Sparse Core Ops, SparseCore 0:
  162.6 118.5 all-gather.12
  283.6 51.7 all-gather.8
  337.1 70.7 all-gather.14
  409.5 44.9 all-gather.10
  464.2 40.8 reduce-scatter.1
where the time goes:
time: 547 us; the launch traced here: 539 us
  waiting for transfers between devices  205 us (37%)
  blocking collectives  165 us (30%)
  local copies, waits for them, and re-layouts  67.4 us (12%)
  matrix products  46.5 us (9%)
  other arithmetic  26.2 us (5%)
  between operations  16.3 us (3%)
  starting transfers between devices  12.9 us (2%)
    all_gather x1, waiting for transfers between devices, shards(): lax.all_gather(arrived, 'tp', axis=0, tiled=True)  116 us
    all_to_all x1, blocking collectives, shards(): lax.all_to_all(outgoing, EP, split_axis=1, concat_axis=1, tiled=True)  108 us
    all_gather x1, waiting for transfers between devices, shards(): lax.all_gather(hidden, 'tp', axis=3, tiled=True)  43.1 us
    all_gather x3, blocking collectives, entering_2(): pieces = jax.tree.map(lambda part: lax.all_gather(part, axis), subtotal)  28.6 us
    scatter x1, local copies, waits for them, and re-layouts, gather_slots(): jnp.zeros((slot_count, expert_count), jnp.int32).at[slot_ids, chosen]  25.4 us
    reduce_scatter x1, waiting for transfers between devices, shards(): lax.psum_scatter(jnp.dot(mixed_heads, out_weight, preferred_element_type=...  19.6 us
    all_gather x1, waiting for transfers between devices, entering_2(): pieces = jax.tree.map(lambda part: lax.all_gather(part, axis), subtotal)  19 us
    all_gather x1, blocking collectives, shards(): lax.all_gather(shared_hidden, 'tp', axis=1, tiled=True)  16.4 us
  transfers between devices with their start and end apart: 6, of which 6 were waited for; matrix products, arithmetic and copies ran while one was open for 12% of the time, Pallas kernels for 0%

commit v1 on v0

v1 whole, which is shorter than its diff:
```python
import jax
import jax.numpy as jnp
from jax import lax
from jax.sharding import Mesh
from jax.sharding import PartitionSpec as P

HD = 128
BLK = 64
CAP = 12
EP = ("ep_0", "ep_1", "ep_2")
PLANE = ("ep_1", "ep_2")
EP_TP = ("ep_0", "ep_1", "ep_2", "tp")
NORM_EPS = 1e-06
ROPE_BASE = 10000.0
EXACT_MATMUL = lax.Precision.HIGHEST


def norm_rows(inputs, gain_vector):
    values = inputs.astype(jnp.float32)
    scaled = values * lax.rsqrt(jnp.mean(values * values, axis=-1, keepdims=True) + NORM_EPS)
    return (scaled * gain_vector).astype(jnp.bfloat16)


def rotate(head_rows, positions):
    head_size = head_rows.shape[-1]
    inverse = ROPE_BASE ** (-jnp.arange(0, head_size, 2, dtype=jnp.float32) / head_size)
    angles = positions[:, None] * inverse[None, :]
    cosine = jnp.cos(angles)[:, None, :]
    sine_part = jnp.sin(angles)[:, None, :]
    front_half = head_rows[..., : head_size // 2]
    behind = head_rows[..., head_size // 2 :]
    return jnp.concatenate(
        [front_half * cosine - behind * sine_part, front_half * sine_part + behind * cosine],
        axis=-1,
    )


def project(inputs, weight, head_total):
    product = jnp.dot(inputs, weight, preferred_element_type=jnp.float32).astype(jnp.bfloat16)
    product = lax.optimization_barrier(product)
    return product.astype(jnp.float32).reshape(inputs.shape[0], head_total, -1)


def entering_state(summary, log_gamma, length):
    planes, members = lax.axis_size("ep_0"), lax.axis_size(PLANE)
    z, j = lax.axis_index("ep_0"), lax.axis_index(PLANE)
    heads = summary.shape[0]
    per_head = members // heads
    sliced = summary.reshape(members, HD // per_head, HD)
    theirs = lax.all_to_all(sliced, PLANE, split_axis=0, concat_axis=0, tiled=True)
    rate = jnp.where(jnp.arange(heads) == j // per_head, log_gamma, 0.0).sum() * length
    spots = jnp.arange(members, dtype=jnp.float32)
    total = jnp.sum(jnp.exp(rate * (members - 1.0 - spots))[:, None, None] * theirs, axis=0)
    totals = lax.all_gather(total, "ep_0")
    plane_ids = jnp.arange(planes)
    before = jnp.where(
        plane_ids < z, jnp.exp(rate * members * jnp.maximum(z - 1 - plane_ids, 0)), 0.0
    )
    passed = jnp.sum(before[:, None, None] * totals, axis=0)
    gaps = spots[:, None] - 1.0 - spots[None, :]
    mix = jnp.where(gaps >= 0, jnp.exp(rate * jnp.maximum(gaps, 0.0)), 0.0)
    inside = jnp.einsum("ij,jab->iab", mix, theirs, precision=EXACT_MATMUL)
    mine = inside + jnp.exp(rate * spots)[:, None, None] * passed[None]
    back = lax.all_to_all(mine, PLANE, split_axis=0, concat_axis=0, tiled=True)
    return back.reshape(summary.shape)


def retain_local(query_heads, key_heads, value_heads, decay_rates):
    length, head_total, head_size = query_heads.shape
    blocks = length // BLK
    log_gamma = -decay_rates
    inner_pos = jnp.arange(BLK, dtype=jnp.float32)
    offsets = inner_pos[:, None] - inner_pos[None, :]
    inside_block_output = jnp.where(
        offsets >= 0, jnp.exp(log_gamma[:, None, None] * jnp.maximum(offsets, 0.0)), 0.0
    )
    key_scale = jnp.exp(log_gamma[None, :] * (BLK - 1.0 - inner_pos)[:, None])
    query_scale = jnp.exp(log_gamma[None, :] * (inner_pos + 1.0)[:, None])
    blocked = (blocks, BLK, head_total, head_size)
    q_blocks = query_heads.reshape(blocked)
    k_blocks = key_heads.reshape(blocked)
    v_blocks = value_heads.reshape(blocked)
    block_states = jnp.einsum(
        "nchd,nche->nhde", k_blocks * key_scale[None, :, :, None], v_blocks, precision=EXACT_MATMUL
    )
    block_offset_rows = jnp.arange(blocks, dtype=jnp.float32)
    to_end = jnp.exp(log_gamma[None, :] * BLK * (blocks - 1.0 - block_offset_rows)[:, None])
    summary = jnp.einsum("nh,nhde->hde", to_end, block_states, precision=EXACT_MATMUL)
    incoming = entering_state(summary, log_gamma, float(length))
    attention_scores = (
        jnp.einsum("nchd,nmhd->nhcm", q_blocks, k_blocks, precision=EXACT_MATMUL)
        * inside_block_output[None]
    )
    nearby = jnp.einsum("nhcm,nmhe->nche", attention_scores, v_blocks, precision=EXACT_MATMUL)
    block_gaps = block_offset_rows[:, None] - 1.0 - block_offset_rows[None, :]
    carry_mix = jnp.where(
        block_gaps >= 0, jnp.exp(log_gamma[:, None, None] * BLK * jnp.maximum(block_gaps, 0.0)), 0.0
    )
    entering = jnp.einsum("hbj,jhde->bhde", carry_mix, block_states, precision=EXACT_MATMUL)
    entering = (
        entering
        + jnp.exp(log_gamma[None, :] * BLK * block_offset_rows[:, None])[:, :, None, None]
        * incoming[None]
    )
    distant = jnp.einsum(
        "bchd,bhde->bche",
        q_blocks * query_scale[None, :, :, None],
        entering,
        precision=EXACT_MATMUL,
    )
    retained = (nearby + distant).reshape(length, head_total, head_size)
    normed = retained * lax.rsqrt(jnp.mean(retained * retained, axis=-1, keepdims=True) + NORM_EPS)
    return normed.astype(jnp.bfloat16).reshape(length, head_total * head_size)


def shards(
    mixer_input,
    expert_input,
    mixer_gain,
    expert_gain,
    query_weight,
    key_weight,
    value_weight,
    out_weight,
    decay_rate,
    routing,
    route_weight,
    gate_weight,
    up_weight,
    down_weight,
    shared_gate,
    shared_up,
    shared_down,
):
    own_count, width = mixer_input.shape
    tp_index = lax.axis_index("tp")
    experts = lax.axis_size(EP)

    own_mixer = norm_rows(mixer_input, mixer_gain)
    own_rows = norm_rows(expert_input, expert_gain)
    mixer_rows = lax.all_gather(own_mixer, "tp", axis=0, tiled=True)
    gates, ups, downs = (
        lax.all_gather(w[0], "tp") for w in (gate_weight, up_weight, down_weight)
    )
    expert_rows = lax.all_gather(own_rows, "tp", axis=0, tiled=True)

    routes = lax.dynamic_slice_in_dim(routing, tp_index * own_count, own_count, 0)
    scales = lax.dynamic_slice_in_dim(route_weight, tp_index * own_count, own_count, 0)
    hits = routes[:, :, None] == jnp.arange(experts, dtype=jnp.int32)[None, None, :]
    member = jnp.any(hits, axis=1)
    weight = jnp.sum(jnp.where(hits, scales[:, :, None], 0.0), axis=1)
    rows = jnp.arange(own_count)
    lower = (rows[None, :] < rows[:, None]).astype(jnp.bfloat16)
    rank = jnp.dot(lower, member.astype(jnp.bfloat16), preferred_element_type=jnp.float32)
    rank = jnp.where(member, rank, -1.0)
    slots = jnp.arange(CAP, dtype=jnp.float32)
    picks = rank.T[:, None, :] == slots[None, :, None]
    sent = jnp.dot(
        picks.astype(jnp.bfloat16).reshape(experts * CAP, own_count),
        own_rows,
        preferred_element_type=jnp.float32,
    ).astype(jnp.bfloat16)
    arrived = lax.all_to_all(sent, EP, split_axis=0, concat_axis=0, tiled=True)

    group_count = mixer_rows.shape[0]
    head_total = decay_rate.shape[0]
    positions = (
        lax.axis_index(EP) * group_count + jnp.arange(group_count, dtype=jnp.int32)
    ).astype(jnp.float32)
    query_heads = rotate(project(mixer_rows, query_weight, head_total), positions) * HD ** (-0.5)
    key_heads = rotate(project(mixer_rows, key_weight, head_total), positions)
    value_heads = project(mixer_rows, value_weight, head_total)
    mixed_heads = retain_local(query_heads, key_heads, value_heads, decay_rate)
    mixer_output = lax.psum_scatter(
        jnp.dot(mixed_heads, out_weight, preferred_element_type=jnp.float32).astype(jnp.bfloat16),
        "tp",
        scatter_dimension=0,
        tiled=True,
    ).astype(jnp.float32)

    gate_part = jnp.einsum("sd,tdf->stf", arrived, gates, preferred_element_type=jnp.float32)
    up_part = jnp.einsum("sd,tdf->stf", arrived, ups, preferred_element_type=jnp.float32)
    hidden = (jax.nn.silu(gate_part) * up_part).astype(jnp.bfloat16).reshape(arrived.shape[0], -1)
    results = jnp.einsum("sf,tfe->ste", hidden, downs, preferred_element_type=jnp.float32)
    results = results.astype(jnp.bfloat16).reshape(arrived.shape[0], width)
    returned = lax.all_to_all(results, EP, split_axis=0, concat_axis=0, tiled=True)
    spread = jnp.where(picks, weight.T[:, None, :], 0.0).reshape(experts * CAP, own_count)
    high = spread.astype(jnp.bfloat16)
    low = (spread - high.astype(jnp.float32)).astype(jnp.bfloat16)
    summed = jnp.einsum("st,sd->td", high, returned, preferred_element_type=jnp.float32)
    summed = summed + jnp.einsum("st,sd->td", low, returned, preferred_element_type=jnp.float32)
    turned = lax.all_to_all(summed, "tp", split_axis=1, concat_axis=0, tiled=True)

    shared_hidden = (
        jax.nn.silu(jnp.dot(expert_rows, shared_gate, preferred_element_type=jnp.float32))
        * jnp.dot(expert_rows, shared_up, preferred_element_type=jnp.float32)
    ).astype(jnp.bfloat16)
    full_shared = lax.all_gather(shared_hidden, "tp", axis=1, tiled=True)
    shared_result = jnp.dot(full_shared, shared_down, preferred_element_type=jnp.float32)
    return (mixer_output, turned + shared_result)


def solution(mesh):
    finer = Mesh(mesh.devices.reshape(8, 4, 2, mesh.shape["tp"]), ("ep_0", "ep_1", "ep_2", "tp"))
    placed = (
        P(EP_TP, None),
        P(EP_TP, None),
        P(),
        P(),
        P(None, "tp"),
        P(None, "tp"),
        P(None, "tp"),
        P("tp", None),
        P("tp"),
        P(EP, None),
        P(EP, None),
        P(EP, None, "tp"),
        P(EP, None, "tp"),
        P(EP, None, "tp"),
        P(None, "tp"),
        P(None, "tp"),
        P(None, "tp"),
    )
    return jax.shard_map(
        shards,
        mesh=finer,
        in_specs=placed,
        out_specs=(P(EP_TP, None), P(EP, "tp")),
        check_vma=False,
    )
```

time: 547 us -> 417 us (0.76)
  waiting for transfers between devices: 205 us -> 114 us
  blocking collectives: 165 us -> 124 us
  local copies, waits for them, and re-layouts: 67.4 us -> 42.7 us
  starting transfers between devices: 12.9 us -> 36.9 us
  matrix products: 46.5 us -> 64.6 us
  other arithmetic: 26.2 us -> 12.8 us
    all_gather x4 -> x5, waiting for transfers between devices: 185 us -> 29 us  [the longest x1 28.9 us: shards(): mixer_rows = lax.all_gather(own_mixer, 'tp', axis=0, tiled=True)]
    all_to_all x1 -> x0, blocking collectives: 108 us -> none  [shards(): lax.all_to_all(outgoing, EP, split_axis=1, concat_axis=1, tiled=True)]
    all_to_all x1 -> x5, waiting for transfers between devices: 0.6 us -> 82.3 us  [the longest x1 82.3 us: shards(): lax.all_to_all(results, EP, split_axis=0, concat_axis=0, tiled=True)]
    all_gather x4 -> x2, blocking collectives: 45 us -> 124 us  [the longest x1 107 us: entering_state(): totals = lax.all_gather(total, 'ep_0')]
    scatter x1 -> x0, local copies, waits for them, and re-layouts: 25.4 us -> none  [gather_slots(): jnp.zeros((slot_count, expert_count), jnp.int32).at[slot_ids, chosen]]
    all_to_all x1 -> x5, starting transfers between devices: 12.5 us -> 36.7 us  [the longest x1 10.7 us: shards(): arrived = lax.all_to_all(sent, EP, split_axis=0, concat_axis=0, tiled=True)]
    dot_general x3 -> x8, matrix products: 19.4 us -> 39.4 us  [the longest x1 9.04 us: shards(): jnp.einsum('sd,tdf->stf', arrived, gates, preferred_element_type=jnp.floa...]
    reduce_scatter x1, waiting for transfers between devices: 19.6 us -> 0.01 us  [shards(): lax.psum_scatter(jnp.dot(mixed_heads, out_weight, preferred_element_type=...]
  transfers between devices with their start and end apart: 6 -> 11, of which waited for: 6 -> 2; matrix products, arithmetic and copies ran while one was open for 12% -> 25% of each run, Pallas kernels for 0% -> 0%
where the time goes in v1:
time: 417 us; the launch traced here: 411 us
  blocking collectives  124 us (30%)
  waiting for transfers between devices  114 us (27%)
  matrix products  64.6 us (15%)
  local copies, waits for them, and re-layouts  42.7 us (10%)
  starting transfers between devices  36.9 us (9%)
  between operations  16.1 us (4%)
  other arithmetic  12.8 us (3%)
    all_gather x1, blocking collectives, entering_state(): totals = lax.all_gather(total, 'ep_0')  107 us
    all_to_all x1, waiting for transfers between devices, shards(): lax.all_to_all(results, EP, split_axis=0, concat_axis=0, tiled=True)  82.3 us
    all_gather x1, waiting for transfers between devices, shards(): mixer_rows = lax.all_gather(own_mixer, 'tp', axis=0, tiled=True)  28.9 us
    all_gather x1, blocking collectives, shards(): full_shared = lax.all_gather(shared_hidden, 'tp', axis=1, tiled=True)  17.2 us
    convert_element_type x1, local copies, waits for them, and re-layouts, shards(): results = results.astype(jnp.bfloat16).reshape(arrived.shape[0], width)  14.8 us
    all_to_all x2, local copies, waits for them, and re-layouts, shards(): arrived = lax.all_to_all(sent, EP, split_axis=0, concat_axis=0, tiled=True)  12.5 us
    all_to_all x1, starting transfers between devices, shards(): arrived = lax.all_to_all(sent, EP, split_axis=0, concat_axis=0, tiled=True)  10.7 us
    all_to_all x1, starting transfers between devices, shards(): lax.all_to_all(results, EP, split_axis=0, concat_axis=0, tiled=True)  9.87 us
  transfers between devices with their start and end apart: 11, of which 2 were waited for; matrix products, arithmetic and copies ran while one was open for 25% of the time, Pallas kernels for 0%

profile of v1, /device:TPU:1, one launch (start us, length us, event | category | flops | bytes accessed | tf_op | source)
XLA Modules:
  0.0 410.6 jit_solution(754294835377227024)
XLA Ops:
  7.2 1.3 fusion.6
  8.6 2.0 fusion.8
  10.7 0.7 all-gather.11.cloned.1.call-update
  11.5 0.7 all-gather.9.cloned.1.call-update
  12.2 0.7 constant_dynamic-slice_fusion.1
  13.1 0.6 copy-done.9
  13.7 0.8 eq.54
  16.1 0.7 exponential_multiply_fusion
  16.8 1.8 multiply_cosine_fusion
  18.8 28.9 %all-gather.7.cloned.1.call-done = bf16[512,2048]{1,0:T(8,128)(2,1)} async-done(((bf16[128,2048]{1,0:T(8,128)(2,1)}), bf16[512,2048]{1,0:T(8,128)(2,1)}) %all-gather.7.cloned.1.call-update) | async-done | bytes 2097168 | tf_op jit(solution)/shard_map/all_gather | solution.py:141
  47.7 2.6 convolution_convert_fusion.4
  50.6 2.6 convolution_convert_fusion.3
  53.4 2.6 convolution_convert_fusion.5
  56.1 1.1 fusion.70
  57.2 1.2 multiply_subtract_fusion.1
  58.6 1.1 fusion.17
  59.7 2.1 fusion.13
  61.8 5.1 %all-to-all-start = ((f32[8,32,128]{2,1,0:T(8,128)}), f32[8,32,128]{2,1,0:T(8,128)S(1)}, u32[]{:S(2)}, u32[]{:S(2)}) async-start(f32[8,32,128]{2,1,0:T(8,128)} %bitcast.93), calls=%async_computation | async-start | bytes 262144 | tf_op jit(solution)/shard_map/all_to_all | solution.py:50
  67.0 3.7 convolution_convert_fusion
  70.7 6.1 %all_to_all.36 = bf16[64,12,2048]{2,1,0:T(8,128)(2,1)} reshape(bf16[768,2048]{1,0:T(8,128)(2,1)} %convolution_convert_fusion) | data formatting | bytes 6291456 | tf_op jit(solution)/shard_map/all_to_all | solution.py:163
  76.8 10.7 %all-to-all-start.2 = ((bf16[64,12,2048]{2,1,0:T(8,128)(2,1)}), bf16[64,12,2048]{2,1,0:T(8,128)(2,1)}, u32[]{:S(2)}, u32[]{:S(2)}) async-start(bf16[64,12,2048]{2,1,0:T(8,128)(2,1)} %all_to_all.36), calls=%async_computation.3 | async-start | bytes 8388608 | tf_op jit(solution)/shard_map/all_to_all | solution.py:163
  89.5 106.6 %all-gather = f32[256,128]{1,0:T(8,128)S(1)} all-gather(f32[32,128]{1,0:T(8,128)S(1)} %multiply_reduce_fusion.2), channel_id=2, replica_groups=mesh['ep_0'=8,'ep_1'=4,'ep_2'=2,'tp'=4] {'ep_0'}, dimensions={0}, use_global_device_ids=true | all-gather | bytes 147456 | tf_op jit(solution)/shard_map/all_gather | solution.py:54
  196.4 0.7 copy.150
  197.1 7.4 %all-to-all-start.1 = ((f32[8,32,128]{2,1,0:T(8,128)}), f32[8,32,128]{2,1,0:T(8,128)S(1)}, u32[]{:S(2)}, u32[]{:S(2)}) async-start(f32[8,32,128]{2,1,0:T(8,128)} %copy.150), calls=%async_computation.1 | async-start | bytes 262144 | tf_op jit(solution)/shard_map/all_to_all | solution.py:64
  204.6 6.4 %reshape.337 = bf16[768,2048,1]{1,0,2:T(8,128)(2,1)} reshape(bf16[64,12,2048]{2,1,0:T(8,128)(2,1)} %all-to-all-done.2) | data formatting | bytes 6291456 | tf_op jit(solution)/shard_map/all_to_all | solution.py:163
  211.0 8.3 %fusion.72 = f32[768,4,256]{0,2,1:T(8,128)} fusion(bf16[768,2048,1]{1,0,2:T(8,128)(2,1)} %reshape.337, bf16[4,2048,256]{2,1,0:T(8,128)(2,1)} %all-gather.11.cloned.1.call-done), kind=kOutput, calls=%fused_computation.131 | convolution fusion | flops 3221225472 | bytes 10485760 | tf_op jit(solution)/shard_map/sd,tdf->stf/dot_general | solution.py:182
  219.3 9.0 %multiply_convert_fusion = bf16[768,4,256]{0,2,1:T(8,128)(2,1)} fusion(f32[768,4,256]{0,2,1:T(8,128)} %fusion.72, bf16[768,2048,1]{1,0,2:T(8,128)(2,1)} %reshape.337, bf16[4,2048,256]{2,1,0:T(8,128)(2,1)} %all-gather.9.cloned.1.call-done), kind=kOutput, calls=%fused_computation.1 | convolution fusion | flops 3225944064 | bytes 12058624 | tf_op jit(solution)/shard_map/sd,tdf->stf/dot_general | solution.py:181
  228.3 6.1 %convolution_convert_fusion.2 = bf16[768,4,512]{2,0,1:T(8,128)(2,1)S(1)} fusion(bf16[768,1024,1]{0,1,2:T(8,128)(2,1)} %bitcast.97, bf16[4,1024,512]{2,1,0:T(8,128)(2,1)} %all-gather.13.cloned.1.call-done), kind=kOutput, calls=%fused_computation.6 | convolution fusion | flops 3222798336 | bytes 8912896 | tf_op jit(solution)/shard_map/sf,tfe->ste/dot_general | solution.py:184
  234.5 14.8 %copy.159 = bf16[768,4,512]{2,1,0:T(4,128)(2,1)} copy(bf16[768,4,512]{2,0,1:T(8,128)(2,1)S(1)} %convolution_convert_fusion.2) | data formatting | bytes 6291456 | tf_op jit(solution)/shard_map/convert_element_type | solution.py:185
  249.3 7.7 %all_to_all.39 = bf16[64,12,2048]{2,1,0:T(8,128)(2,1)} reshape(bf16[768,4,512]{2,1,0:T(4,128)(2,1)} %copy.159) | data formatting | bytes 6291456 | tf_op jit(solution)/shard_map/all_to_all | solution.py:186
  257.0 9.9 %all-to-all-start.3 = ((bf16[64,12,2048]{2,1,0:T(8,128)(2,1)}), bf16[64,12,2048]{2,1,0:T(8,128)(2,1)}, u32[]{:S(2)}, u32[]{:S(2)}) async-start(bf16[64,12,2048]{2,1,0:T(8,128)(2,1)} %all_to_all.39), calls=%async_computation.4 | async-start | bytes 8388608 | tf_op jit(solution)/shard_map/all_to_all | solution.py:186
  267.6 0.8 fusion.58
  268.4 0.7 fusion.57
  269.2 2.1 convolution_multiply_fusion
  271.7 2.3 fusion.3
  274.0 1.3 multiply_reduce_fusion
  276.5 2.1 convolution_convert_fusion.1
  278.6 0.7 constant_dynamic-slice_fusion
  279.3 82.3 %all-to-all-done.3 = bf16[64,12,2048]{2,1,0:T(8,128)(2,1)} async-done(((bf16[64,12,2048]{2,1,0:T(8,128)(2,1)}), bf16[64,12,2048]{2,1,0:T(8,128)(2,1)}, u32[]{:S(2)}, u32[]{:S(2)}) %all-to-all-start.3) | async-done | bytes 3145760 | tf_op jit(solution)/shard_map/all_to_all | solution.py:186
  361.6 5.8 %convolution_bitcast_fusion = f32[128,2048]{1,0:T(8,128)S(1)} fusion(bf16[64,12,2048]{2,1,0:T(8,128)(2,1)} %all-to-all-done.3, f32[64,128]{1,0:T(8,128)S(1)} %bitcast.94, f32[64,128]{1,0:T(8,128)S(1)} %copy-done.10), kind=kOutput, calls=%fused_computation.3 | convolution fusion | flops 403243008 | bytes 4259840 | tf_op jit(solution)/shard_map/st,sd->td/dot_general | solution.py:191
  367.4 6.0 %fusion = f32[128,2048]{1,0:T(8,128)S(1)} fusion(f32[128,2048]{1,0:T(8,128)S(1)} %convolution_bitcast_fusion, bf16[64,12,2048]{2,1,0:T(8,128)(2,1)} %all-to-all-done.3, f32[64,128]{1,0:T(8,128)S(1)} %bitcast.95, f32[64,128]{1,0:T(8,128)S(1)} %copy-done.10), kind=kOutput, calls=%fused_computation.5 | convolution fusion | flops 403111936 | bytes 5308416 | tf_op jit(solution)/shard_map/st,sd->td/dot_general | solution.py:190
  373.5 1.0 copy.234
  374.5 3.5 all-to-all-start.4
  378.1 2.3 fusion.73
  380.4 2.4 fusion.5
  382.8 17.2 %all_gather.31 = bf16[512,512]{1,0:T(8,128)(2,1)S(1)} all-gather(bf16[512,128]{1,0:T(8,128)(2,1)S(1)} %fusion.5), channel_id=1, replica_groups=mesh['ep_0'=8,'ep_1'=4,'ep_2'=2,'tp'=4] {'tp'}, dimensions={1}, use_global_device_ids=true | all-gather | bytes 655360 | tf_op jit(solution)/shard_map/all_gather | solution.py:198
  400.0 2.1 convert_element_type.85
  402.2 1.4 convolution_add_fusion
  (83 shorter events, 6.4 us)
Async XLA Ops:
  7.2 269.3 %copy-start = (bf16[256,2048]{1,0:T(8,128)(2,1)S(1)}, bf16[256,2048]{1,0:T(8,128)(2,1)}, u32[]{:S(2)}) copy-start(bf16[256,2048]{1,0:T(8,128)(2,1)} %param.24) | copy-start | bytes 3145732
  7.2 7.5 %copy-start.4 = (bf16[128,2048]{1,0:T(8,128)(2,1)S(1)}, bf16[128,2048]{1,0:T(8,128)(2,1)}, u32[]{:S(2)}) copy-start(bf16[128,2048]{1,0:T(8,128)(2,1)} %param.18) | copy-start | bytes 1572868
  7.2 7.7 %copy-start.14 = (f32[2]{0:T(128)S(1)}, f32[2]{0:T(128)}, u32[]{:S(2)}) copy-start(f32[2]{0:T(128)} %param.25) | copy-start | bytes 28
  7.2 40.5 %all-gather.7.cloned.1.call-start = ((), (), s32[]{:S(2)}) async-start(), calls=%async_computation.6 | async-start | bytes 2621440 | tf_op jit(solution)/shard_map/all_gather | solution.py:141
  8.6 10.0 %copy-start.11 = (f32[2048]{0:T(1024)S(1)}, f32[2048]{0:T(1024)}, u32[]{:S(2)}) copy-start(f32[2048]{0:T(1024)} %param.20) | copy-start | bytes 24580
  10.7 200.3 %all-gather.11.cloned.1.call-start = ((), (), s32[]{:S(2)}) async-start(), calls=%async_computation.9 | async-start | bytes 5242880 | tf_op jit(solution)/shard_map/all_gather | solution.py:143
  11.4 207.9 %all-gather.9.cloned.1.call-start = ((), (), s32[]{:S(2)}) async-start(), calls=%async_computation.8 | async-start | bytes 5242880 | tf_op jit(solution)/shard_map/all_gather | solution.py:143
  13.1 0.6 copy-start.9
  18.8 48.2 %copy-start.1 = (bf16[128,2048]{1,0:T(8,128)(2,1)}, bf16[128,2048]{1,0:T(8,128)(2,1)S(1)}, u32[]{:S(2)}) copy-start(bf16[128,2048]{1,0:T(8,128)(2,1)S(1)} %fusion.11) | copy-start | bytes 1572868
  56.0 1.2 copy-start.5
  56.1 1.2 copy-start.6
  61.8 14.9 %all-to-all-start = ((f32[8,32,128]{2,1,0:T(8,128)}), f32[8,32,128]{2,1,0:T(8,128)S(1)}, u32[]{:S(2)}, u32[]{:S(2)}) async-start(f32[8,32,128]{2,1,0:T(8,128)} %bitcast.93), calls=%async_computation | async-start | bytes 262144 | tf_op jit(solution)/shard_map/all_to_all | solution.py:50
  76.8 120.4 %all-to-all-start.2 = ((bf16[64,12,2048]{2,1,0:T(8,128)(2,1)}), bf16[64,12,2048]{2,1,0:T(8,128)(2,1)}, u32[]{:S(2)}, u32[]{:S(2)}) async-start(bf16[64,12,2048]{2,1,0:T(8,128)(2,1)} %all_to_all.36), calls=%async_computation.3 | async-start | bytes 8388608 | tf_op jit(solution)/shard_map/all_to_all | solution.py:163
  87.5 140.8 %all-gather.13.cloned.1.call-start = ((), (), s32[]{:S(2)}) async-start(), calls=%async_computation.10 | async-start | bytes 5242880 | tf_op jit(solution)/shard_map/all_gather | solution.py:143
  89.4 121.6 %copy-start.13 = (f32[8]{0:T(128)}, f32[8]{0:T(128)S(1)}, u32[]{:S(2)}) copy-start(f32[8]{0:T(128)S(1)} %iota_add_fusion.1) | copy-start | bytes 100
  197.1 59.9 %all-to-all-start.1 = ((f32[8,32,128]{2,1,0:T(8,128)}), f32[8,32,128]{2,1,0:T(8,128)S(1)}, u32[]{:S(2)}, u32[]{:S(2)}) async-start(f32[8,32,128]{2,1,0:T(8,128)} %copy.150), calls=%async_computation.1 | async-start | bytes 262144 | tf_op jit(solution)/shard_map/all_to_all | solution.py:64
  257.0 12.1 %copy-start.2 = (f32[512,2,64]{2,0,1:T(8,128)S(1)}, f32[512,2,64]{2,0,1:T(8,128)}, u32[]{:S(2)}) copy-start(f32[512,2,64]{2,0,1:T(8,128)} %get-tuple-element.2) | copy-start | bytes 786436
  257.0 104.6 %all-to-all-start.3 = ((bf16[64,12,2048]{2,1,0:T(8,128)(2,1)}), bf16[64,12,2048]{2,1,0:T(8,128)(2,1)}, u32[]{:S(2)}, u32[]{:S(2)}) async-start(bf16[64,12,2048]{2,1,0:T(8,128)(2,1)} %all_to_all.39), calls=%async_computation.4 | async-start | bytes 8388608 | tf_op jit(solution)/shard_map/all_to_all | solution.py:186
  266.9 7.0 %copy-start.12 = (f32[64,2]{0,1:T(2,128)S(1)}, f32[64,2]{0,1:T(2,128)}, u32[]{:S(2)}) copy-start(f32[64,2]{0,1:T(2,128)} %get-tuple-element.14) | copy-start | bytes 1540
  266.9 111.1 %all-gather.15.cloned.1.call-start = ((), (), s32[]{:S(2)}) async-start(), calls=%async_computation.11 | async-start | bytes 2621440 | tf_op jit(solution)/shard_map/all_gather | solution.py:145
  267.5 132.5 %reduce-scatter.2.cloned.1.call-start = ((), (), s32[]{:S(2)}) async-start(), calls=%async_computation.7 | async-start | bytes 2621440 | tf_op jit(solution)/shard_map/reduce_scatter | solution.py:174
  267.5 6.4 %copy-start.3 = (f32[512,2,64]{2,0,1:T(8,128)S(1)}, f32[512,2,64]{2,0,1:T(8,128)}, u32[]{:S(2)}) copy-start(f32[512,2,64]{2,0,1:T(8,128)} %get-tuple-element.3) | copy-start | bytes 786436
  276.5 85.1 %copy-start.10 = (f32[64,128]{1,0:T(8,128)S(1)}, f32[64,128]{1,0:T(8,128)}, u32[]{:S(2)}) copy-start(f32[64,128]{1,0:T(8,128)} %copy-done.9) | copy-start | bytes 98308
  373.4 4.6 %copy-start.7 = (bf16[2048,128]{1,0:T(8,128)(2,1)S(1)}, bf16[2048,128]{1,0:T(8,128)(2,1)}, u32[]{:S(2)}) copy-start(bf16[2048,128]{1,0:T(8,128)(2,1)} %param.31) | copy-start | bytes 1572868
  374.5 27.7 %all-to-all-start.4 = ((f32[128,4,512]{2,0,1:T(8,128)}), f32[128,4,512]{2,0,1:T(8,128)S(1)}, u32[]{:S(2)}, u32[]{:S(2)}) async-start(f32[128,4,512]{2,0,1:T(8,128)} %bitcast.79), calls=%async_computation.5 | async-start | bytes 2097152 | tf_op jit(solution)/shard_map/all_to_all | solution.py:192
  380.4 21.8 %copy-start.8 = (bf16[512,512]{1,0:T(8,128)(2,1)S(1)}, bf16[512,512]{1,0:T(8,128)(2,1)}, u32[]{:S(2)}) copy-start(bf16[512,512]{1,0:T(8,128)(2,1)} %param.33) | copy-start | bytes 1572868
Sparse Core Ops, SparseCore 0:
  10.8 36.9 all-gather.6
  49.5 50.7 all-gather.10
  102.2 51.0 all-gather.8
  155.0 51.0 all-gather.12
  269.2 32.8 all-gather.14
  304.5 32.3 reduce-scatter.1
